TPU v7x, 128 devices: a whole 4x4x4 slice. The times are simulated.
128 devices in a mesh: sp: 64 (over z, y, x), tp: 2 (over core).
Axes of the slice: x: 4, y: 4, z: 4, core: 2. Of those that a mesh axis runs over, the one named last changes fastest.
Arguments:
- queries: bfloat16 [16384, 1024], P('sp', 'tp'), may hold values from -6 to 6
- keys: bfloat16 [16384, 256], P('sp', 'tp'), may hold values from -6 to 6
- values: bfloat16 [16384, 256], P('sp', 'tp'), may hold values from -24 to 24
- sink_logit: float32 [16], P('tp'), may hold values from 3 to 7
- w_out: bfloat16 [1024, 2048], replicated, may hold values from -0.1875 to 0.1875
- residual: bfloat16 [16384, 2048], P(('sp', 'tp')), may hold values from -3 to 3
- norm_gain: float32 [2048], replicated, may hold values from 0.1 to 1.9
- w_gate: bfloat16 [64, 2048, 2048], P('sp', None, 'tp'), may hold values from -0.5 to 0.5
- w_up: bfloat16 [64, 2048, 2048], P('sp', None, 'tp'), may hold values from -0.5 to 0.5
- w_down: bfloat16 [64, 2048, 2048], P('sp', 'tp'), may hold values from -0.125 to 0.125
- expert_ids: int32 [16384, 2], P(('sp', 'tp')), may hold values from 0 to 63, all different within a row; in each aligned block of 128 rows (0 to 127, 128 to 255, ...) at most 6 rows name the same one
- route_weight: float32 [16384, 2], P(('sp', 'tp')), may hold values from 0.2 to 1
Outputs:
- final: bfloat16 [16384, 2048], P(('sp', 'tp'))
Inputs may be any that keep to these rules, and one draw needn't show every extreme that they name: `expert_ids`: in the rows of one device each row names 2 different experts and no expert is named by more than 6 rows; some expert is named by exactly 6 of them.
All inputs are finite; a program needn't handle non-finite values.
Results may differ from a plain program's by a relative error of at most 0.0097.
Values may be sent and summed in bfloat16 or wider, within the bound.
A program may use at most 128 MiB of HBM per device.

v0:
```python
import jax
import jax.numpy as jnp
from jax import lax
from jax.sharding import PartitionSpec as P

HEAD_DIM = 64
WINDOW = 128


CLAMP_LIMIT = 7.0
GATE_ALPHA = 1.702
EPSILON = 1e-06
NEG_BIG = -1e30


def with_halo(shard, sides, width):
    for axis, dim in sides:
        devices, length = (lax.axis_size(axis), shard.shape[dim])
        up = [(i, (i + 1) % devices) for i in range(devices - 1)]
        down = [(j, i) for i, j in up]
        last = lax.slice_in_dim(shard, length - width, length, axis=dim)
        leading = lax.slice_in_dim(shard, 0, width, axis=dim)
        before = lax.ppermute(last, axis, up)
        after = lax.ppermute(leading, axis, down)
        shard = jnp.concatenate([before, shard, after], axis=dim)
    return shard


def split_up(shard, dim, devices):
    before, after = (shard.shape[:dim], shard.shape[dim + 1 :])
    return jnp.moveaxis(shard.reshape(*before, devices, -1, *after), dim, 0)


def summed_on_arrival(shard, axis, dim):
    parts = split_up(shard, dim, lax.axis_size(axis))
    arrived = lax.all_to_all(parts, axis, split_axis=0, concat_axis=0, tiled=True)
    return arrived.sum(axis=0)


def in_order(parts, dim):
    parts = jnp.moveaxis(parts, 0, dim)
    lengths = parts.shape
    return parts.reshape(*lengths[:dim], lengths[dim] * lengths[dim + 1], *lengths[dim + 2 :])


def sent_to_all(shard, axis):
    devices = lax.axis_size(axis)
    return lax.all_to_all(
        jnp.broadcast_to(shard[None], (devices, *shard.shape)), axis, 0, 0, tiled=True
    )


def gather_directly(shard, axis, dim):
    return in_order(sent_to_all(shard, axis), dim)


def summed_on_arrival_2(shard, axis, dim):
    devices = lax.axis_size(axis)
    parts = lax.all_to_all(split_up(shard, dim, devices), axis, 0, 0, tiled=True)
    return jnp.sum(parts.astype(jnp.float32), axis=0)


def attend(queries, keys_vals, sink_logit, offset, seq_total, groups):
    span_rows = queries.shape[0]
    local_heads = queries.shape[1] // HEAD_DIM
    repeat = local_heads // groups
    q_block = min(512, span_rows)
    logit_sink = sink_logit.reshape(groups, repeat)[:, :, None, None]
    query_block = queries.reshape(q_block, groups, repeat, HEAD_DIM)
    key_block = keys_vals[0, 0 : q_block + 2 * WINDOW].reshape(
        q_block + 2 * WINDOW, groups, HEAD_DIM
    )
    value_block = keys_vals[1, 0 : q_block + 2 * WINDOW].reshape(
        q_block + 2 * WINDOW, groups, HEAD_DIM
    )
    scores = jnp.einsum(
        "qgrd,kgd->grqk", query_block, key_block, preferred_element_type=jnp.float32
    ) * HEAD_DIM ** (-0.5)
    query_pos = offset + 0 + jnp.arange(q_block, dtype=jnp.int32)
    key_pos = offset + 0 - WINDOW + jnp.arange(q_block + 2 * WINDOW, dtype=jnp.int32)
    key_gap = key_pos[None, :] - query_pos[:, None]
    in_window = (
        (jnp.abs(key_gap) <= WINDOW) & (key_pos[None, :] >= 0) & (key_pos[None, :] < seq_total)
    )
    scores = jnp.where(in_window, scores, NEG_BIG)
    peak = jnp.maximum(jnp.max(scores, axis=-1, keepdims=True), logit_sink)
    expo = jnp.exp(scores - peak)
    divisor = jnp.sum(expo, axis=-1, keepdims=True) + jnp.exp(logit_sink - peak)
    softmax_w = (expo / divisor).astype(jnp.bfloat16)
    mixed = jnp.einsum("grqk,kgd->qgrd", softmax_w, value_block, preferred_element_type=jnp.float32)
    pieces = mixed.reshape(q_block, local_heads * HEAD_DIM).astype(jnp.bfloat16)
    return pieces


def per_device(
    queries,
    keys,
    values,
    sink_logit,
    w_out,
    residual,
    norm_gain,
    w_gate,
    w_up,
    w_down,
    expert_ids,
    route_weight,
):
    span_rows = queries.shape[0]
    sp_size = lax.axis_size("sp")
    offset = lax.axis_index("sp") * span_rows
    stacked = jnp.stack([keys, values])
    padded = with_halo(stacked, (("sp", 1),), WINDOW)
    groups = keys.shape[1] // HEAD_DIM
    attended = attend(queries, padded, sink_logit, offset, span_rows * sp_size, groups)
    pair_size = lax.axis_size("tp")
    own_count = span_rows // pair_size
    head_cols = attended.shape[1]
    own_rows = lax.dynamic_slice_in_dim(w_out, lax.axis_index("tp") * head_cols, head_cols, 0)
    projected = summed_on_arrival(
        jnp.dot(attended, own_rows, preferred_element_type=jnp.float32), "tp", 0
    )
    attn_proj = lax.optimization_barrier(projected.astype(jnp.bfloat16))
    midway = residual.astype(jnp.float32) + attn_proj.astype(jnp.float32)
    normed = (
        midway * lax.rsqrt(jnp.mean(midway * midway, axis=-1, keepdims=True) + EPSILON) * norm_gain
    ).astype(jnp.bfloat16)
    width_model = normed.shape[1]
    expert_count = w_gate.shape[0] * sp_size
    top_count = expert_ids.shape[1]
    capacity = 3 * own_count * top_count // (2 * expert_count)
    chosen = expert_ids.reshape(-1)
    onehot = (chosen[:, None] == jnp.arange(expert_count, dtype=jnp.int32)[None, :]).astype(
        jnp.int32
    )
    earlier = jnp.cumsum(onehot, axis=0) - onehot
    slot_ids = (chosen * capacity + jnp.sum(earlier * onehot, axis=1)).reshape(own_count, top_count)
    slot_table = jnp.any(
        slot_ids[None, :, :] == jnp.arange(expert_count * capacity, dtype=jnp.int32)[:, None, None],
        axis=2,
    ).astype(jnp.bfloat16)
    buffer = (
        jnp.dot(slot_table, normed, preferred_element_type=jnp.float32)
        .astype(jnp.bfloat16)
        .reshape(expert_count, capacity, width_model)
    )
    arrived = lax.all_to_all(buffer, "sp", split_axis=0, concat_axis=0, tiled=True)
    rows_in = gather_directly(arrived[None], "tp", 0)
    in_shape = rows_in.shape
    flat_rows = rows_in.reshape(-1, in_shape[-1])
    gate_pre = jnp.dot(flat_rows, w_gate[0], preferred_element_type=jnp.float32)
    up_pre = jnp.dot(flat_rows, w_up[0], preferred_element_type=jnp.float32)
    act_clip = jnp.minimum(gate_pre, CLAMP_LIMIT)
    up_clip = jnp.clip(up_pre, -CLAMP_LIMIT, CLAMP_LIMIT)
    hidden = ((up_clip + 1.0) * act_clip * jax.nn.sigmoid(GATE_ALPHA * act_clip)).astype(
        jnp.bfloat16
    )
    down_part = jnp.dot(hidden, w_down[0], preferred_element_type=jnp.float32)
    terms = down_part.reshape(in_shape)
    summed = summed_on_arrival_2(terms.astype(jnp.bfloat16), "tp", 0)[0].astype(jnp.bfloat16)
    merged = lax.all_to_all(summed, "sp", split_axis=0, concat_axis=0, tiled=True)
    flat_out = merged.reshape(expert_count * capacity, width_model)
    picked = jnp.take(flat_out, slot_ids, axis=0)
    routed = jnp.sum(picked.astype(jnp.float32) * route_weight[:, :, None], axis=1)
    return (midway + routed).astype(jnp.bfloat16)


def solution(mesh):
    in_specs = (
        P("sp", "tp"),
        P("sp", "tp"),
        P("sp", "tp"),
        P("tp"),
        P(),
        P(("sp", "tp"), None),
        P(),
        P("sp", None, "tp"),
        P("sp", None, "tp"),
        P("sp", "tp", None),
        P(("sp", "tp"), None),
        P(("sp", "tp"), None),
    )
    out_specs = P(("sp", "tp"), None)
    return jax.shard_map(
        per_device, mesh=mesh, in_specs=in_specs, out_specs=out_specs, check_vma=False
    )
```

profile of v0, /device:TPU:1, one launch (start us, length us, event | category | flops | bytes accessed | tf_op | source)
XLA Modules:
  0.0 170.5 jit_solution(893028559766776116)
XLA Ops:
  0.8 3.9 %collective-permute-start = (bf16[2,128,128]{2,1,0:T(8,128)(2,1)S(1)}, bf16[2,128,128]{2,1,0:T(8,128)(2,1)S(1)}, u32[]{:S(2)}, u32[]{:S(2)}) collective-permute-start(bf16[2,128,128]{2,1,0:T(8,128)(2,1)S(1)} %get-tuple-element.9), channel_id=1, source_target_pairs={{0,2},{2,4},{4,6},{6,8},{8,10},{10,12},{12,14},{14,16},{16,18},{18... | collective-permute-start | bytes 196616 | tf_op jit(solution)/shard_map/ppermute | solution.py:23
  4.8 1.3 collective-permute-start.1
  13.2 1.8 %copy-done = f32[2,512,256,4]{2,1,3,0:T(8,128)} copy-done((f32[2,512,256,4]{2,1,3,0:T(8,128)}, f32[2,512,256,4]{2,1,3,0:T(8,128)S(1)}, u32[]{:S(2)}) %copy-start) | copy-done | bytes 4194328
  16.1 3.4 %fusion.22 = bf16[256,2,4,64]{0,3,2,1:T(8,128)(2,1)S(1)} fusion(bf16[512,2,64,1]{0,2,3,1:T(8,128)(2,1)S(1)} %bitcast.93, f32[2,512,256,4]{2,1,3,0:T(8,128)} %copy-done, f32[2,4,256]{2,1,0:T(4,128)S(1)} %exponential_add_fusion, f32[2,4,256]{2,1,0:T(4,128)S(1)} %broadcast_maximum_fusion, pred[256,512]{0,1:T(8,128)(4,1)S(1)} %fusion.26), kind=kOutput, calls=%fused_computation.25 | convolution fusion | flops 139591680 | bytes 4734976 | tf_op jit(solution)/shard_map/grqk,kgd->qgrd/dot_general | solution.py:90
  19.6 2.3 %fusion.14 = f32[2,128,2048]{2,1,0:T(8,128)S(1)} fusion(bf16[1024,2048]{1,0:T(8,128)(2,1)} %param.16, s32[]{:T(128)S(6)} %select_n.17, bf16[2,128,512]{1,0,2:T(2,128)(2,1)S(1)} %convert_element_type.54), kind=kOutput, calls=%fused_computation.17 | convolution fusion | flops 536870912 | bytes 4456452 | tf_op jit(solution)/shard_map/dot_general | solution.py:121
  22.0 6.1 %all_to_all.25 = f32[2,128,2048]{2,1,0:T(8,128)S(1)} all-to-all(f32[2,128,2048]{2,1,0:T(8,128)S(1)} %fusion.14), channel_id=1, replica_groups=mesh['sp'=64,'tp'=2] {'tp'}, dimensions={0} | all-to-all | bytes 4194304 | tf_op jit(solution)/shard_map/all_to_all | solution.py:36
  28.6 1.8 %convolution_convert_fusion = bf16[384,2048]{1,0:T(8,128)(2,1)} fusion(pred[384,128]{1,0:T(8,128)(4,1)S(1)} %fusion.27, bf16[128,2048]{1,0:T(8,128)(2,1)S(1)} %reduce_sum.60, bf16[128,2048]{1,0:T(8,128)(2,1)S(1)} %copy-done.1, f32[2048]{0:T(1024)S(1)} %copy-done.3, f32[128]{0:T(128)S(1)} %add_rsqrt_fusion), kind=kOutput, calls=%fused_computation.16 | convolution fusion | flops 203685888 | bytes 2679296 | tf_op jit(solution)/shard_map/dot_general | solution.py:143
  30.4 2.5 %reshape.100 = bf16[64,6,2048]{2,1,0:T(8,128)(2,1)S(1)} reshape(bf16[384,2048]{1,0:T(8,128)(2,1)} %convolution_convert_fusion) | data formatting | bytes 3145728 | tf_op jit(solution)/shard_map/reshape | solution.py:145
  32.9 42.9 %all_to_all.26 = bf16[64,6,2048]{2,1,0:T(8,128)(2,1)S(1)} all-to-all(bf16[64,6,2048]{2,1,0:T(8,128)(2,1)S(1)} %reshape.100), channel_id=1, replica_groups=mesh['sp'=64,'tp'=2] {'sp'}, dimensions={0} | all-to-all | bytes 3145728 | tf_op jit(solution)/shard_map/all_to_all | solution.py:147
  77.0 8.0 %all_to_all.27 = bf16[2,1,64,6,2048]{4,2,3,1,0:T(8,128)(2,1)S(1)} all-to-all(bf16[2,1,64,6,2048]{4,2,3,1,0:T(8,128)(2,1)S(1)} %broadcast_in_dim.39), channel_id=1, replica_groups=mesh['sp'=64,'tp'=2] {'tp'}, dimensions={0} | all-to-all | bytes 6291456 | tf_op jit(solution)/shard_map/all_to_all | solution.py:48
  85.0 3.7 %copy.97 = bf16[2,1,64,6,2048]{4,3,2,0,1:T(8,128)(2,1)} copy(bf16[2,1,64,6,2048]{4,2,3,1,0:T(8,128)(2,1)S(1)} %all_to_all.27) | data formatting | bytes 6291456 | tf_op jit(solution)/shard_map/all_to_all | solution.py:48
  88.7 6.3 %reshape_reshape.3 = bf16[768,2048]{1,0:T(8,128)(2,1)} reshape(bf16[2,1,64,6,2048]{4,3,2,0,1:T(8,128)(2,1)} %copy.97) | data formatting | bytes 6291456 | tf_op jit(solution)/shard_map/reshape;reshape | solution.py:150
  95.1 6.3 %fusion.2 = f32[768,1024]{1,0:T(8,128)S(1)} fusion(bf16[768,2048]{1,0:T(8,128)(2,1)} %reshape_reshape.3, bf16[1,2048,1024]{2,1,0:T(8,128)(2,1)} %param.19), kind=kOutput, calls=%fused_computation.3 | convolution fusion | flops 3221225472 | bytes 10485760 | tf_op jit(solution)/shard_map/dot_general | solution.py:151
  101.4 5.3 %multiply_convert_fusion = bf16[768,1024]{1,0:T(8,128)(2,1)} fusion(f32[768,1024]{1,0:T(8,128)S(1)} %fusion.2, bf16[768,2048]{1,0:T(8,128)(2,1)S(1)} %copy-done.2, bf16[1,2048,1024]{2,1,0:T(8,128)(2,1)S(1)} %copy-done.5), kind=kOutput, calls=%fused_computation.14 | convolution fusion | flops 3229089792 | bytes 12058624 | tf_op jit(solution)/shard_map/dot_general | solution.py:152
  106.6 2.5 %dot_general.29 = bf16[2,64,6,1024]{3,2,1,0:T(8,128)(2,1)S(1)} reshape(bf16[768,1024]{1,0:T(8,128)(2,1)} %multiply_convert_fusion) | data formatting | bytes 3145728 | tf_op jit(solution)/shard_map/dot_general | solution.py:158
  109.1 6.0 %fusion.11 = bf16[2,1,64,6,2048]{4,2,3,1,0:T(8,128)(2,1)S(1)} fusion(bf16[1,1024,2048]{2,1,0:T(8,128)(2,1)} %param.21, bf16[2,64,6,1024]{3,2,1,0:T(8,128)(2,1)S(1)} %dot_general.29), kind=kOutput, calls=%fused_computation.15 | convolution fusion | flops 3222798336 | bytes 8912896 | tf_op jit(solution)/shard_map/dot_general | solution.py:158
  115.1 6.2 %all_to_all.28 = bf16[2,1,64,6,2048]{4,2,3,1,0:T(8,128)(2,1)S(1)} all-to-all(bf16[2,1,64,6,2048]{4,2,3,1,0:T(8,128)(2,1)S(1)} %fusion.11), channel_id=1, replica_groups=mesh['sp'=64,'tp'=2] {'tp'}, dimensions={0} | all-to-all | bytes 6291456 | tf_op jit(solution)/shard_map/all_to_all | solution.py:59
  122.0 2.2 %copy.101 = bf16[64,6,2048]{2,1,0:T(8,128)(2,1)} copy(bf16[64,6,2048]{2,0,1:T(8,128)(2,1)S(1)} %bitcast_reduce_fusion) | data formatting | bytes 3145728 | tf_op jit(solution)/shard_map/reduce_sum | solution.py:60
  124.2 5.9 %all-to-all-start.4 = ((bf16[64,6,2048]{2,1,0:T(8,128)(2,1)}), bf16[64,6,2048]{2,1,0:T(8,128)(2,1)}, u32[]{:S(2)}, u32[]{:S(2)}) async-start(bf16[64,6,2048]{2,1,0:T(8,128)(2,1)} %copy.101), calls=%async_computation.4 | async-start | bytes 4194304 | tf_op jit(solution)/shard_map/all_to_all | solution.py:161
  130.6 28.1 %all-to-all-done.4 = bf16[64,6,2048]{2,1,0:T(8,128)(2,1)} async-done(((bf16[64,6,2048]{2,1,0:T(8,128)(2,1)}), bf16[64,6,2048]{2,1,0:T(8,128)(2,1)}, u32[]{:S(2)}, u32[]{:S(2)}) %all-to-all-start.4) | async-done | bytes 1572896 | tf_op jit(solution)/shard_map/all_to_all | solution.py:161
  158.7 2.6 %reshape.102 = bf16[384,2048]{1,0:T(8,128)(2,1)S(1)} reshape(bf16[64,6,2048]{2,1,0:T(8,128)(2,1)} %all-to-all-done.4) | data formatting | bytes 3145728 | tf_op jit(solution)/shard_map/reshape | solution.py:162
  161.3 2.3 %gather_fusion = bf16[256,2048]{1,0:T(8,128)(2,1)} fusion(bf16[384,2048]{1,0:T(8,128)(2,1)S(1)} %reshape.102, s32[1024]{0:T(1024)S(1)} %pad_clamp_fusion), kind=kCustom, calls=%fused_computation | custom fusion | bytes 2098176 | tf_op jit(solution)/shard_map/jit(_take)/gather | solution.py:163
  163.6 1.7 %reshape.104 = bf16[128,2,2048]{2,1,0:T(2,128)(2,1)S(1)} reshape(bf16[256,2048]{1,0:T(8,128)(2,1)} %gather_fusion) | data formatting | bytes 2097152 | tf_op jit(solution)/shard_map/jit(_take)/gather | solution.py:163
  165.4 4.1 %multiply_reduce_fusion = f32[128,2048]{1,0:T(8,128)S(1)} fusion(bf16[128,2,2048]{2,1,0:T(2,128)(2,1)S(1)} %reshape.104, pred[128,2]{1,0:T(8,128)(4,1)S(1)} %copy.95, f32[128,2]{1,0:T(8,128)S(1)} %copy.103), kind=kLoop, calls=%fused_computation.19 | loop fusion | flops 1835008 | bytes 2098432 | tf_op jit(solution)/shard_map/reduce_sum | solution.py:164
  (55 shorter events, 12.9 us)
Async XLA Ops:
  0.8 10.4 %collective-permute-start = (bf16[2,128,128]{2,1,0:T(8,128)(2,1)S(1)}, bf16[2,128,128]{2,1,0:T(8,128)(2,1)S(1)}, u32[]{:S(2)}, u32[]{:S(2)}) collective-permute-start(bf16[2,128,128]{2,1,0:T(8,128)(2,1)S(1)} %get-tuple-element.9), channel_id=1, source_target_pairs={{0,2},{2,4},{4,6},{6,8},{8,10},{10,12},{12,14},{14,16},{16,18},{18... | collective-permute-start | bytes 196616 | tf_op jit(solution)/shard_map/ppermute | solution.py:23
  4.8 6.5 %collective-permute-start.1 = (bf16[2,128,128]{2,1,0:T(8,128)(2,1)S(1)}, bf16[2,128,128]{2,1,0:T(8,128)(2,1)S(1)}, u32[]{:S(2)}, u32[]{:S(2)}) collective-permute-start(bf16[2,128,128]{2,1,0:T(8,128)(2,1)S(1)} %get-tuple-element.10), channel_id=1, source_target_pairs={{2,0},{4,2},{6,4},{8,6},{10,8},{12,10},{14,12},{16,14},{18,16},{20... | collective-permute-start | bytes 196616 | tf_op jit(solution)/shard_map/ppermute | solution.py:24
  13.1 1.9 %copy-start = (f32[2,512,256,4]{2,1,3,0:T(8,128)}, f32[2,512,256,4]{2,1,3,0:T(8,128)S(1)}, u32[]{:S(2)}) copy-start(f32[2,512,256,4]{2,1,3,0:T(8,128)S(1)} %get-tuple-element.12) | copy-start | bytes 12582916
  21.9 6.3 %copy-start.1 = (bf16[128,2048]{1,0:T(8,128)(2,1)S(1)}, bf16[128,2048]{1,0:T(8,128)(2,1)}, u32[]{:S(2)}) copy-start(bf16[128,2048]{1,0:T(8,128)(2,1)} %param.17) | copy-start | bytes 1572868
  21.9 6.6 %copy-start.3 = (f32[2048]{0:T(1024)S(1)}, f32[2048]{0:T(1024)}, u32[]{:S(2)}) copy-start(f32[2048]{0:T(1024)} %param.18) | copy-start | bytes 24580
  95.1 6.3 %copy-start.2 = (bf16[768,2048]{1,0:T(8,128)(2,1)S(1)}, bf16[768,2048]{1,0:T(8,128)(2,1)}, u32[]{:S(2)}) copy-start(bf16[768,2048]{1,0:T(8,128)(2,1)} %reshape_reshape.3) | copy-start | bytes 9437188
  95.1 6.3 %copy-start.5 = (bf16[1,2048,1024]{2,1,0:T(8,128)(2,1)S(1)}, bf16[1,2048,1024]{2,1,0:T(8,128)(2,1)}, u32[]{:S(2)}) copy-start(bf16[1,2048,1024]{2,1,0:T(8,128)(2,1)} %param.20) | copy-start | bytes 12582916
  122.0 8.5 %copy-start.4 = (f32[128,2]{0,1:T(2,128)S(1)}, f32[128,2]{0,1:T(2,128)}, u32[]{:S(2)}) copy-start(f32[128,2]{0,1:T(2,128)} %param.23) | copy-start | bytes 3076
  124.2 34.5 %all-to-all-start.4 = ((bf16[64,6,2048]{2,1,0:T(8,128)(2,1)}), bf16[64,6,2048]{2,1,0:T(8,128)(2,1)}, u32[]{:S(2)}, u32[]{:S(2)}) async-start(bf16[64,6,2048]{2,1,0:T(8,128)(2,1)} %copy.101), calls=%async_computation.4 | async-start | bytes 4194304 | tf_op jit(solution)/shard_map/all_to_all | solution.py:161
where the time goes:
time: 172 us; the launch traced here: 170 us
  blocking collectives  63.2 us (37%)
  local copies, waits for them, and re-layouts  31.1 us (18%)
  waiting for transfers between devices  28.1 us (16%)
  matrix products  25.9 us (15%)
  starting transfers between devices  11.1 us (6%)
  other arithmetic  10.8 us (6%)
    all_to_all x1, blocking collectives, per_device(): lax.all_to_all(buffer, 'sp', split_axis=0, concat_axis=0, tiled=True)  42.9 us
    all_to_all x1, waiting for transfers between devices, per_device(): lax.all_to_all(summed, 'sp', split_axis=0, concat_axis=0, tiled=True)  28.1 us
    all_to_all x1, blocking collectives, sent_to_all(): lax.all_to_all(jnp.broadcast_to(shard[None], (devices, *shard.shape)), ax...  8.01 us
    another operation x1, local copies, waits for them, and re-layouts, per_device(): flat_rows = rows_in.reshape(-1, in_shape[-1])  6.33 us
    dot_general x1, matrix products, per_device(): gate_pre = jnp.dot(flat_rows, w_gate[0], preferred_element_type=jnp.float32)  6.28 us
    all_to_all x1, blocking collectives, summed_on_arrival_2(): lax.all_to_all(split_up(shard, dim, devices), axis, 0, 0, tiled=True)  6.2 us
    all_to_all x1, blocking collectives, summed_on_arrival(): lax.all_to_all(parts, axis, split_axis=0, concat_axis=0, tiled=True)  6.13 us
    dot_general x1, matrix products, per_device(): down_part = jnp.dot(hidden, w_down[0], preferred_element_type=jnp.float32)  5.97 us
  transfers between devices with their start and end apart: 3, of which 1 were waited for; matrix products, arithmetic and copies ran while one was open for 3% of the time, Pallas kernels for 0%

commit v1 on v0

v1 whole, which is shorter than its diff:
```python
import functools
import random

import jax
import jax.numpy as jnp
from jax import lax
from jax.experimental import pallas as pl
from jax.experimental.pallas import tpu as pltpu
from jax.sharding import PartitionSpec as P

MESH = pl.DeviceIdType.MESH
BF = jnp.bfloat16
F32 = jnp.float32

NSP = 64
WIN = 128
DM = 2048
HID = 1024
SLOT = 6
PAD = 8
WAVES = 4
PER = NSP // WAVES
HALF = PER * PAD
ROWS = 2 * HALF
CLAMP_LIMIT = 7.0
GATE_ALPHA = 1.702
EPSILON = 1e-06
NEG_BIG = -1e30
EXP_SCALE = 1.4426950408889634 / 8.0


def offsets():
    every = [(a, b, c) for a in range(4) for b in range(4) for c in range(4)]
    seen, groups = {(0, 0, 0)}, []
    for o in every:
        if o in seen:
            continue
        group = []
        for p in ((0, 1, 2), (1, 2, 0), (2, 0, 1)):
            for s in (1, -1):
                m = tuple((s * o[i]) % 4 for i in p)
                if m not in group:
                    group.append(m)
        seen |= set(group)
        groups.append(group)
    random.Random(1).shuffle(groups)
    groups.sort(key=lambda g: -sum(min(v, 4 - v) for v in g[0]))
    return [(0, 0, 0)] + [o for g in groups for o in g]


ORDER = offsets()


def shifted(me, off, sign):
    z, y, x = me // 16, (me // 4) % 4, me % 4
    dz, dy, dx = [(sign * v) % 4 for v in off]
    return ((z + dz) % 4) * 16 + ((y + dy) % 4) * 4 + (x + dx) % 4


def body(
    q_hbm, k_hbm, v_hbm, sink, wout_hbm, res_hbm, gain_hbm, wg_hbm, wu_hbm, wd_hbm, ids_hbm, rw_hbm,
    out,
    q_v, kv, kmask, vmask, bias, att, attx, wout, res, gain, wg, wu, wd, ids, rw,
    midway, normed, disp, comb, xbuf3, xin3, hid, part, recv, back3, ret3,
    local_sem, halo_s, halo_r, att_s, att_r, d_s, d_r, f_s, f_r, p_s, p_r, r_s, r_r,
):
    me = lax.axis_index("sp")
    t = lax.axis_index("tp")
    other = 1 - t
    xbuf, back, ret = [b.reshape(NSP * PAD, DM) for b in (xbuf3, back3, ret3)]
    xin = xin3.reshape(WAVES * ROWS, DM)
    right = lax.rem(me + 1, NSP)
    left = lax.rem(me + NSP - 1, NSP)

    barrier = pltpu.get_barrier_semaphore()

    @pl.loop(1, NSP)
    def _(i):
        pl.semaphore_signal(
            barrier, inc=1, device_id=(lax.rem(me + i, NSP), t), device_id_type=MESH
        )

    pl.semaphore_signal(barrier, inc=1, device_id=(me, other), device_id_type=MESH)

    loads = [
        (k_hbm, kv.at[0, pl.ds(WIN, 2 * WIN)]),
        (v_hbm, kv.at[1, pl.ds(WIN, 2 * WIN)]),
        (q_hbm, q_v),
        (ids_hbm, ids),
        (rw_hbm, rw),
        (wout_hbm, wout),
        (res_hbm, res),
        (gain_hbm, gain),
        (wg_hbm, wg),
        (wu_hbm, wu),
        (wd_hbm, wd),
    ]
    copies = [
        pltpu.make_async_copy(a, b, local_sem.at[i]) for i, (a, b) in enumerate(loads)
    ]
    for c in copies:
        c.start()

    ret[...] = jnp.zeros_like(ret)

    copies[3].wait()
    copies[4].wait()
    sub = lax.broadcasted_iota(jnp.int32, (NSP, WIN), 0)
    ohs = [(sub == ids[k : k + 1, :]).astype(F32) for k in range(2)]
    before = (
        lax.broadcasted_iota(jnp.int32, (WIN, WIN), 0)
        < lax.broadcasted_iota(jnp.int32, (WIN, WIN), 1)
    ).astype(BF)
    total0 = jnp.sum(ohs[0], axis=1, keepdims=True)
    slot_rows = []
    for k in range(2):
        earlier = jnp.dot(ohs[k].astype(BF), before, preferred_element_type=F32)
        if k == 1:
            earlier = earlier + total0
        rank = jnp.sum(ohs[k] * earlier, axis=0, keepdims=True)
        slot_rows.append(ids[k : k + 1, :] * PAD + rank.astype(jnp.int32))
    srow = lax.broadcasted_iota(jnp.int32, (NSP * PAD, WIN), 0)
    hits = [srow == slot_rows[k] for k in range(2)]
    disp[...] = (hits[0] | hits[1]).astype(F32).astype(BF)
    weight = jnp.where(hits[0], rw[0:1, :], 0.0) + jnp.where(hits[1], rw[1:2, :], 0.0)
    weight = weight.T
    high = weight.astype(BF)
    comb[0] = high
    comb[1] = (weight - high.astype(F32)).astype(BF)

    copies[0].wait()
    copies[1].wait()
    pl.semaphore_wait(barrier, NSP)
    to_left = pltpu.make_async_remote_copy(
        kv.at[:, pl.ds(WIN, WIN)], kv.at[:, pl.ds(3 * WIN, WIN)], halo_s.at[0], halo_r.at[0],
        device_id=(left, t), device_id_type=MESH,
    )
    to_right = pltpu.make_async_remote_copy(
        kv.at[:, pl.ds(2 * WIN, WIN)], kv.at[:, pl.ds(0, WIN)], halo_s.at[1], halo_r.at[1],
        device_id=(right, t), device_id_type=MESH,
    )
    to_left.start()
    to_right.start()

    row = lax.broadcasted_iota(jnp.int32, (WIN, WIN), 0)
    col = lax.broadcasted_iota(jnp.int32, (WIN, WIN), 1)
    bias[0] = jnp.where(col >= row, 0.0, NEG_BIG)
    bias[1] = jnp.where(col <= row, 0.0, NEG_BIG)
    copies[2].wait()
    to_left.wait()
    to_right.wait()

    low = lax.broadcasted_iota(jnp.int32, (4 * WIN, WIN), 1) < 64
    keys = kv[0].astype(F32)
    keys_r = pltpu.roll(keys, 64, 1)
    vals = kv[1].astype(F32)
    vals_r = pltpu.roll(vals, 64, 1)
    ones = jnp.ones_like(keys)
    for g in range(2):
        k_lo, k_hi = (keys, keys_r) if g == 0 else (keys_r, keys)
        v_lo, v_hi = (vals, vals_r) if g == 0 else (vals_r, vals)
        kmask[g, 0] = jnp.where(low, k_lo, 0.0).astype(BF)
        kmask[g, 1] = jnp.where(low, 0.0, k_hi).astype(BF)
        vmask[g, 0, :, 0:WIN] = jnp.where(low, v_lo, 0.0).astype(BF)
        vmask[g, 1, :, 0:WIN] = jnp.where(low, 0.0, v_hi).astype(BF)
        vmask[g, 0, :, WIN:] = jnp.where(low, ones, 0.0).astype(BF)
        vmask[g, 1, :, WIN:] = jnp.where(low, 0.0, ones).astype(BF)

    lane_low = lax.broadcasted_iota(jnp.int32, (WIN, WIN), 1) < 64

    def tile(step, _):
        qt = lax.rem(other + step, 2)
        base = pl.multiple_of(qt * WIN, WIN)
        no_left = jnp.where((me == 0) & (qt == 0), NEG_BIG, 0.0).astype(F32)
        no_right = jnp.where((me == NSP - 1) & (qt == 1), NEG_BIG, 0.0).astype(F32)
        bias_l = bias[0] + no_left
        bias_r = bias[1] + no_right
        for pair in range(4):
            g = pair // 2
            qp = q_v[pl.ds(base, WIN), pair * WIN : (pair + 1) * WIN]
            acc = None
            tail = []
            for side in range(2):
                s = lax.dot_general(
                    qp, kmask[g, side, pl.ds(base, 3 * WIN), :], (((1,), (1,)), ((), ())),
                    preferred_element_type=F32,
                )
                s_l = s[:, 0:WIN] + bias_l
                s_m = s[:, WIN : 2 * WIN]
                s_r = s[:, 2 * WIN :] + bias_r
                logit = sink[2 * pair + side] * 8.0
                peak = jnp.max(
                    jnp.maximum(jnp.maximum(s_l, s_m), s_r), axis=1, keepdims=True
                )
                peak = jnp.maximum(peak, logit)
                expo = jnp.concatenate(
                    [jnp.exp2((v - peak) * EXP_SCALE).astype(BF) for v in (s_l, s_m, s_r)],
                    axis=1,
                )
                o = jnp.dot(
                    expo, vmask[g, side, pl.ds(base, 3 * WIN), :], preferred_element_type=F32
                )
                acc = o if acc is None else acc + o
                tail.append(jnp.exp2((logit - peak) * EXP_SCALE))
            div = acc[:, WIN:] + jnp.where(lane_low, tail[0], tail[1])
            att[pl.ds(base, WIN), pair * WIN : (pair + 1) * WIN] = (
                acc[:, 0:WIN] / div
            ).astype(BF)

        @pl.when(step == 0)
        def _():
            send_att().start()

        return 0

    def send_att():
        return pltpu.make_async_remote_copy(
            att.at[pl.ds(pl.multiple_of(other * WIN, WIN), WIN)], attx, att_s, att_r,
            device_id=(me, other), device_id_type=MESH,
        )

    lax.fori_loop(0, 2, tile, 0)

    copies[5].wait()
    copies[6].wait()
    copies[7].wait()
    send_att().wait()

    mine = pl.multiple_of(t * WIN, WIN)
    w_mine = pl.multiple_of(t * 512, 512)
    w_other = pl.multiple_of(other * 512, 512)
    square = jnp.zeros((WIN, WIN), F32)
    for c in range(8):
        cols = slice(c * 256, (c + 1) * 256)
        proj = jnp.dot(
            att[pl.ds(mine, WIN), :], wout[pl.ds(w_mine, 512), cols], preferred_element_type=F32
        ) + jnp.dot(attx[...], wout[pl.ds(w_other, 512), cols], preferred_element_type=F32)
        mid = res[:, cols].astype(F32) + proj.astype(BF).astype(F32)
        midway[:, cols] = mid
        sq = mid * mid
        square = square + sq[:, 0:WIN] + sq[:, WIN:]
    inv = lax.rsqrt(jnp.sum(square, axis=1, keepdims=True) * (1.0 / DM) + EPSILON)
    for c in range(8):
        cols = slice(c * 256, (c + 1) * 256)
        normed[:, cols] = (midway[:, cols] * inv * gain[:, cols]).astype(BF)
    for c in range(8):
        cols = slice(c * 256, (c + 1) * 256)
        xbuf[:, cols] = jnp.dot(
            disp[...], normed[:, cols], preferred_element_type=F32
        ).astype(BF)

    def wave_rows(w, side):
        return (w * 2 + side) * HALF

    def dispatch(i):
        d = shifted(me, ORDER[i], 1)
        spot = (i // PER * 2 + t) * PER + i % PER
        return pltpu.make_async_remote_copy(
            xbuf3.at[d, pl.ds(0, SLOT)], xin3.at[spot, pl.ds(0, SLOT)],
            d_s.at[i], d_r.at[i], device_id=(d, t), device_id_type=MESH,
        )

    for i in range(1, NSP):
        dispatch(i).start()
    xin[pl.ds(pl.multiple_of(t * HALF, HALF), PAD), :] = xbuf[
        pl.ds(pl.multiple_of(me * PAD, PAD), PAD), :
    ]

    def forward(w):
        rows = pl.ds((w * 2 + t) * PER, PER)
        return pltpu.make_async_remote_copy(
            xin3.at[rows], xin3.at[rows], f_s.at[w], f_r.at[w],
            device_id=(me, other), device_id_type=MESH,
        )

    def halves(w):
        rows = pl.ds(pl.multiple_of(wave_rows(w, other), HALF), HALF)
        return pltpu.make_async_remote_copy(
            part.at[rows], recv.at[pl.ds(w * HALF, HALF)], p_s.at[w], p_r.at[w],
            device_id=(me, other), device_id_type=MESH,
        )

    def give_back(i):
        d = shifted(me, ORDER[i], -1)
        return pltpu.make_async_remote_copy(
            back3.at[i, pl.ds(0, SLOT)], ret3.at[me, pl.ds(0, SLOT)],
            r_s.at[i], r_r.at[i], device_id=(d, t), device_id_type=MESH,
        )

    def arrive(w):
        for i in range(max(1, w * PER), (w + 1) * PER):
            dispatch(i).wait_recv()
        forward(w).start()

    def compute(w):
        forward(w).wait_recv()
        if w == 0:
            copies[8].wait()
            copies[9].wait()
            copies[10].wait()
        rows = slice(w * ROWS, (w + 1) * ROWS)
        for c in range(HID // 256):
            cols = slice(c * 256, (c + 1) * 256)
            gate = jnp.dot(xin[rows, :], wg[:, cols], preferred_element_type=F32)
            up = jnp.dot(xin[rows, :], wu[:, cols], preferred_element_type=F32)
            act = jnp.minimum(gate, CLAMP_LIMIT)
            lin = jnp.clip(up, -CLAMP_LIMIT, CLAMP_LIMIT) + 1.0
            hid[:, cols] = (lin * act * jax.nn.sigmoid(GATE_ALPHA * act)).astype(BF)
        for c in range(DM // 256):
            cols = slice(c * 256, (c + 1) * 256)
            part[rows, cols] = jnp.dot(
                hid[...], wd[:, cols], preferred_element_type=F32
            ).astype(BF)
        halves(w).start()

    def finish(w):
        halves(w).wait_recv()
        own = pl.ds(pl.multiple_of(wave_rows(w, t), HALF), HALF)
        rows = slice(w * HALF, (w + 1) * HALF)
        for c in range(DM // 512):
            cols = slice(c * 512, (c + 1) * 512)
            back[rows, cols] = (
                part[own, cols].astype(F32) + recv[rows, cols].astype(F32)
            ).astype(BF)
        for i in range(max(1, w * PER), (w + 1) * PER):
            give_back(i).start()
        if w == 0:
            ret[pl.ds(pl.multiple_of(me * PAD, PAD), PAD), :] = back[0:PAD, :]

    arrive(0)
    for w in range(WAVES):
        compute(w)
        if w + 1 < WAVES:
            arrive(w + 1)
        finish(w)

    for i in range(1, NSP):
        give_back(i).wait_recv()
    for c in range(8):
        cols = slice(c * 256, (c + 1) * 256)
        routed = jnp.dot(comb[0], ret[:, cols], preferred_element_type=F32) + jnp.dot(
            comb[1], ret[:, cols], preferred_element_type=F32
        )
        out[:, cols] = (midway[:, cols] + routed).astype(BF)

    for i in range(1, NSP):
        dispatch(i).wait_send()
        give_back(i).wait_send()
    for w in range(WAVES):
        forward(w).wait_send()
        halves(w).wait_send()


def per_device(
    queries, keys, values, sink_logit, w_out, residual, norm_gain, w_gate, w_up, w_down,
    expert_ids, route_weight,
):
    any_spec = pl.BlockSpec(memory_space=pl.ANY)
    specs = [any_spec] * 12
    specs[3] = pl.BlockSpec(memory_space=pltpu.SMEM)
    dma = pltpu.SemaphoreType.DMA
    return pl.pallas_call(
        body,
        out_shape=jax.ShapeDtypeStruct((WIN, DM), BF),
        in_specs=specs,
        out_specs=pl.BlockSpec(memory_space=pltpu.VMEM),
        scratch_shapes=[
            pltpu.VMEM((2 * WIN, 512), BF),
            pltpu.VMEM((2, 4 * WIN, WIN), BF),
            pltpu.VMEM((2, 2, 4 * WIN, WIN), BF),
            pltpu.VMEM((2, 2, 4 * WIN, 2 * WIN), BF),
            pltpu.VMEM((2, WIN, WIN), F32),
            pltpu.VMEM((2 * WIN, 512), BF),
            pltpu.VMEM((WIN, 512), BF),
            pltpu.VMEM((1024, DM), BF),
            pltpu.VMEM((WIN, DM), BF),
            pltpu.VMEM((1, DM), F32),
            pltpu.VMEM((DM, HID), BF),
            pltpu.VMEM((DM, HID), BF),
            pltpu.VMEM((HID, DM), BF),
            pltpu.VMEM((2, WIN), jnp.int32),
            pltpu.VMEM((2, WIN), F32),
            pltpu.VMEM((WIN, DM), F32),
            pltpu.VMEM((WIN, DM), BF),
            pltpu.VMEM((NSP * PAD, WIN), BF),
            pltpu.VMEM((2, WIN, NSP * PAD), BF),
            pltpu.VMEM((NSP, PAD, DM), BF),
            pltpu.VMEM((2 * NSP, PAD, DM), BF),
            pltpu.VMEM((ROWS, HID), BF),
            pltpu.VMEM((WAVES * ROWS, DM), BF),
            pltpu.VMEM((NSP * PAD, DM), BF),
            pltpu.VMEM((NSP, PAD, DM), BF),
            pltpu.VMEM((NSP, PAD, DM), BF),
            dma((11,)),
            dma((2,)),
            dma((2,)),
            dma,
            dma,
            dma((NSP,)),
            dma((NSP,)),
            dma((WAVES,)),
            dma((WAVES,)),
            dma((WAVES,)),
            dma((WAVES,)),
            dma((NSP,)),
            dma((NSP,)),
        ],
        compiler_params=pltpu.CompilerParams(
            collective_id=0, has_side_effects=True, vmem_limit_bytes=62 * 2**20
        ),
    )(
        queries, keys, values, sink_logit, w_out, residual, norm_gain.reshape(1, DM),
        w_gate[0], w_up[0], w_down[0], expert_ids.T, route_weight.T,
    )


def solution(mesh):
    in_specs = (
        P("sp", "tp"),
        P("sp", "tp"),
        P("sp", "tp"),
        P("tp"),
        P(),
        P(("sp", "tp"), None),
        P(),
        P("sp", None, "tp"),
        P("sp", None, "tp"),
        P("sp", "tp", None),
        P(("sp", "tp"), None),
        P(("sp", "tp"), None),
    )
    return jax.shard_map(
        per_device,
        mesh=mesh,
        in_specs=in_specs,
        out_specs=P(("sp", "tp"), None),
        check_vma=False,
    )
```

time: 172 us -> 67.9 us (0.39)
  Pallas kernels: 0 us -> 64.9 us
  blocking collectives: 63.2 us -> 0 us
  local copies, waits for them, and re-layouts: 31.1 us -> 1.88 us
  waiting for transfers between devices: 28.1 us -> 0 us
  matrix products: 25.9 us -> 0 us
  starting transfers between devices: 11.1 us -> 0 us
  other arithmetic: 10.8 us -> 0 us
    pallas_call x0 -> x1, Pallas kernels: none -> 64.9 us  [per_device(): pl.pallas_call(body, out_shape=jax.ShapeDtypeStruct((WIN, DM), BF), in_sp...]
    all_to_all x4 -> x0, blocking collectives: 63.2 us -> none  [the longest x1 42.9 us: per_device(): lax.all_to_all(buffer, 'sp', split_axis=0, concat_axis=0, tiled=True)]
    all_to_all x1 -> x0, waiting for transfers between devices: 28.1 us -> none  [per_device(): lax.all_to_all(summed, 'sp', split_axis=0, concat_axis=0, tiled=True)]
    dot_general x7 -> x0, matrix products: 25.9 us -> none  [the longest x1 6.28 us: per_device(): gate_pre = jnp.dot(flat_rows, w_gate[0], preferred_element_type=jnp.float32)]
    another operation x2 -> x0, local copies, waits for them, and re-layouts: 6.34 us -> none  [the longest x1 6.33 us: per_device(): flat_rows = rows_in.reshape(-1, in_shape[-1])]
    reduce_sum x6 -> x0, other arithmetic: 6.18 us -> none  [the longest x1 4.07 us: per_device(): jnp.sum(picked.astype(jnp.float32) * route_weight[:, :, None], axis=1)]
    all_to_all x1 -> x0, starting transfers between devices: 5.91 us -> none  [per_device(): lax.all_to_all(summed, 'sp', split_axis=0, concat_axis=0, tiled=True)]
    ppermute x2 -> x0, starting transfers between devices: 5.23 us -> none  [the longest x1 3.94 us: with_halo(): before = lax.ppermute(last, axis, up)]
  transfers between devices with their start and end apart: 3 -> 0, of which waited for: 1 -> 0; matrix products, arithmetic and copies ran while one was open for 3% -> 0% of each run, Pallas kernels for 0% -> 0%
where the time goes in v1:
time: 67.9 us; the launch traced here: 66.8 us
  Pallas kernels  64.9 us (96%)
  local copies, waits for them, and re-layouts  1.88 us (3%)
    pallas_call x1, Pallas kernels, per_device(): pl.pallas_call(body, out_shape=jax.ShapeDtypeStruct((WIN, DM), BF), in_sp...  64.9 us
    unnamed x1, local copies, waits for them, and re-layouts  1.88 us

profile of v1, /device:TPU:1, one launch (start us, length us, event | category | flops | bytes accessed | tf_op | source)
XLA Modules:
  0.0 66.8 jit_solution(14564735349498220094)
XLA Ops:
  0.0 64.9 %shard_map.118 = bf16[128,2048]{1,0:T(8,128)(2,1)} custom-call(bf16[256,512]{1,0:T(8,128)(2,1)} %q_hbm.1, bf16[256,128]{1,0:T(8,128)(2,1)} %k_hbm.1, bf16[256,128]{1,0:T(8,128)(2,1)} %v_hbm.1, f32[8]{0:T(128)} %sink.1, bf16[1024,2048]{1,0:T(8,128)(2,1)} %wout_hbm.1, bf16[128,2048]{1,0:T(8,128)(2,1)} %res_hbm.1, f32[1,2048]{1,0:T(1,128)} %bitcast.9, ...), custom_call_target="tpu_custom_call" | custom-call | tf_op jit(solution)/shard_map/pallas_call | solution.py:362
  65.0 1.9 %copy.14 = bf16[128,2048]{1,0:T(8,128)(2,1)} copy(bf16[128,2048]{1,0:T(8,128)(2,1)} %shard_map.118) | data formatting | bytes 1048576

commit v2 on v1

v2 whole, which is shorter than its diff:
```python
import functools
import random

import jax
import jax.numpy as jnp
import numpy as np
from jax import lax
from jax.experimental import pallas as pl
from jax.experimental.pallas import tpu as pltpu
from jax.sharding import PartitionSpec as P

MESH = pl.DeviceIdType.MESH
BF = jnp.bfloat16
F32 = jnp.float32

NSP = 64
WIN = 128
DM = 2048
HID = 1024
SLOT = 6
TILE = 8
SIZES = (8, 8, 16, 16, 16)
WAVES = len(SIZES)
PLAN = (
    "a0", "u0", "a1", "d0", "u1", "f0", "a2", "d1", "a3", "u2",
    "f1", "a4", "d2", "u3", "f2", "d3", "u4", "f3", "d4", "f4",
)
FIRST = [sum(SIZES[:w]) for w in range(WAVES)]
MOST = max(SIZES)
SLOTS = NSP * SLOT


def pieces(i):
    at, end = i * SLOT, (i + 1) * SLOT
    while at < end:
        upto = min(end, (at // TILE + 1) * TILE)
        yield at // TILE, at % TILE, upto - at
        at = upto
CLAMP_LIMIT = 7.0
GATE_ALPHA = 1.702
EPSILON = 1e-06
NEG_BIG = -1e30
EXP_SCALE = 1.4426950408889634 / 8.0


def offsets():
    every = [(a, b, c) for a in range(4) for b in range(4) for c in range(4)]
    seen, groups = {(0, 0, 0)}, []
    for o in every:
        if o in seen:
            continue
        group = []
        for p in ((0, 1, 2), (1, 2, 0), (2, 0, 1)):
            for s in (1, -1):
                m = tuple((s * o[i]) % 4 for i in p)
                if m not in group:
                    group.append(m)
        seen |= set(group)
        groups.append(group)
    random.Random(1).shuffle(groups)
    groups.sort(key=lambda g: -sum(min(v, 4 - v) for v in g[0]))
    return [(0, 0, 0)] + [o for g in groups for o in g]


ORDER = offsets()


def shifted(me, off, sign):
    z, y, x = me // 16, (me // 4) % 4, me % 4
    dz, dy, dx = [(sign * v) % 4 for v in off]
    return ((z + dz) % 4) * 16 + ((y + dy) % 4) * 4 + (x + dx) % 4


def body(
    q_hbm, k_hbm, v_hbm, sink_hbm, wout_hbm, res_hbm, gain_hbm, wg_hbm, wu_hbm, wd_hbm, ids_hbm, rw_hbm,
    tab_hbm, out,
    q_v, kv, kmask, vmask, bias, near, peaks, att, attx, sink, wout, res, gain, wg, wu, wd, ids, rw, tab,
    midway, normed, disp, comb, xbuf3, xin3, hid, part, recv, back3, ret3,
    local_sem, halo_s, halo_r, att_s, att_r, d_s, d_r, f_s, f_r, p_s, p_r, r_s, r_r,
):
    me = lax.axis_index("sp")
    t = lax.axis_index("tp")
    other = 1 - t
    xbuf, back, ret = [b.reshape(SLOTS, DM) for b in (xbuf3, back3, ret3)]
    xin = xin3.reshape(2 * SLOTS, DM)
    right = lax.rem(me + 1, NSP)
    left = lax.rem(me + NSP - 1, NSP)

    loads = [
        (k_hbm, kv.at[0, pl.ds(WIN, 2 * WIN)]),
        (v_hbm, kv.at[1, pl.ds(WIN, 2 * WIN)]),
        (q_hbm, q_v),
        (ids_hbm, ids),
        (rw_hbm, rw),
        (wout_hbm, wout),
        (res_hbm, res),
        (gain_hbm, gain),
        (wg_hbm, wg),
        (wu_hbm, wu),
        (wd_hbm, wd),
        (tab_hbm, tab),
        (sink_hbm, sink),
    ]
    copies = [
        pltpu.make_async_copy(a, b, local_sem.at[i]) for i, (a, b) in enumerate(loads)
    ]
    for i in (0, 1, 2, 12, 3, 4, 11, 6, 7, 5, 8, 9, 10):
        copies[i].start()

    barrier = pltpu.get_barrier_semaphore()
    pl.semaphore_signal(barrier, inc=1, device_id=(left, t), device_id_type=MESH)
    pl.semaphore_signal(barrier, inc=1, device_id=(right, t), device_id_type=MESH)
    pl.semaphore_signal(barrier, inc=1, device_id=(me, other), device_id_type=MESH)
    for i in range(2, NSP - 1):
        pl.semaphore_signal(
            barrier, inc=1, device_id=(lax.rem(me + i, NSP), t), device_id_type=MESH
        )

    row = lax.broadcasted_iota(jnp.int32, (WIN, WIN), 0)
    col = lax.broadcasted_iota(jnp.int32, (WIN, WIN), 1)
    for i in (3, 4, 11):
        copies[i].wait()
    ret[...] = jnp.zeros_like(ret)
    sub = lax.broadcasted_iota(jnp.int32, (NSP, WIN), 0)
    ohs = [(sub == ids[k : k + 1, :]).astype(F32) for k in range(2)]
    before = (row < col).astype(F32).astype(BF)
    total0 = jnp.sum(ohs[0], axis=1, keepdims=True)
    slot_rows = []
    for k in range(2):
        earlier = jnp.dot(ohs[k].astype(BF), before, preferred_element_type=F32)
        if k == 1:
            earlier = earlier + total0
        rank = jnp.sum(ohs[k] * earlier, axis=0, keepdims=True)
        slot_rows.append(ids[k : k + 1, :] * SLOT + rank.astype(jnp.int32))
    offs = tab[...] >> 3
    there = (
        ((me // 16 + offs // 16) & 3) * 16
        + (((me // 4) % 4 + offs // 4) & 3) * 4
        + ((me % 4 + offs) & 3)
    )
    srow = there * SLOT + (tab[...] & 7)
    hits = [srow == slot_rows[k] for k in range(2)]
    disp[...] = (hits[0] | hits[1]).astype(F32).astype(BF)

    copies[0].wait()
    copies[1].wait()
    pl.semaphore_wait(barrier, NSP)
    to_left = pltpu.make_async_remote_copy(
        kv.at[:, pl.ds(WIN, WIN)], kv.at[:, pl.ds(3 * WIN, WIN)], halo_s.at[0], halo_r.at[0],
        device_id=(left, t), device_id_type=MESH,
    )
    to_right = pltpu.make_async_remote_copy(
        kv.at[:, pl.ds(2 * WIN, WIN)], kv.at[:, pl.ds(0, WIN)], halo_s.at[1], halo_r.at[1],
        device_id=(right, t), device_id_type=MESH,
    )
    to_left.start()
    to_right.start()

    bias[0] = jnp.where(col >= row, 0.0, NEG_BIG)
    bias[1] = jnp.where(col <= row, 0.0, NEG_BIG)

    def spread(lo, size):
        rows = slice(lo, lo + size)
        low = lax.broadcasted_iota(jnp.int32, (size, WIN), 1) < 64
        keys = kv[0, rows].astype(F32)
        keys_r = pltpu.roll(keys, 64, 1)
        vals = kv[1, rows].astype(F32)
        vals_r = pltpu.roll(vals, 64, 1)
        ones = jnp.ones_like(keys)
        for g in range(2):
            k_lo, k_hi = (keys, keys_r) if g == 0 else (keys_r, keys)
            v_lo, v_hi = (vals, vals_r) if g == 0 else (vals_r, vals)
            kmask[g, 0, rows] = jnp.where(low, k_lo, 0.0).astype(BF)
            kmask[g, 1, rows] = jnp.where(low, 0.0, k_hi).astype(BF)
            vmask[g, 0, rows, 0:WIN] = jnp.where(low, v_lo, 0.0).astype(BF)
            vmask[g, 1, rows, 0:WIN] = jnp.where(low, 0.0, v_hi).astype(BF)
            vmask[g, 0, rows, WIN:] = jnp.where(low, ones, 0.0).astype(BF)
            vmask[g, 1, rows, WIN:] = jnp.where(low, 0.0, ones).astype(BF)

    spread(WIN, 2 * WIN)
    copies[2].wait()
    copies[12].wait()

    lane_low = lax.broadcasted_iota(jnp.int32, (WIN, WIN), 1) < 64

    def scores(qp, keys):
        return lax.dot_general(
            qp, keys, (((1,), (1,)), ((), ())), preferred_element_type=F32
        )

    def own_tile(qt, _):
        base = pl.multiple_of(qt * WIN, WIN)
        cut_a = jnp.where(qt == 1, bias[0], 0.0)
        cut_b = jnp.where(qt == 0, bias[1], 0.0)
        for pair in range(4):
            g = pair // 2
            qp = q_v[pl.ds(base, WIN), pair * WIN : (pair + 1) * WIN]
            acc = None
            for side in range(2):
                s = scores(qp, kmask[g, side, WIN : 3 * WIN, :])
                s_a = s[:, 0:WIN] + cut_a
                s_b = s[:, WIN:] + cut_b
                logit = sink[2 * pair + side] * 8.0
                peak = jnp.max(jnp.maximum(s_a, s_b), axis=1, keepdims=True)
                peak = jnp.maximum(peak, logit)
                expo = jnp.concatenate(
                    [jnp.exp2((v - peak) * EXP_SCALE).astype(BF) for v in (s_a, s_b)], axis=1
                )
                o = jnp.dot(
                    expo, vmask[g, side, WIN : 3 * WIN, :], preferred_element_type=F32
                )
                acc = o if acc is None else acc + o
                peaks[qt, pair, side] = jnp.broadcast_to(peak, (WIN, WIN))
            near[qt, pair] = acc
        return 0

    lax.fori_loop(0, 2, own_tile, 0)

    to_left.wait()
    to_right.wait()
    spread(0, WIN)
    spread(3 * WIN, WIN)

    def far_tile(step, _):
        qt = lax.rem(other + step, 2)
        base = pl.multiple_of(qt * WIN, WIN)
        edge = ((me == 0) & (qt == 0)) | ((me == NSP - 1) & (qt == 1))
        cut = jnp.where(qt == 0, bias[0], bias[1]) + jnp.where(edge, NEG_BIG, 0.0)
        keys_at = pl.ds(pl.multiple_of(qt * 3 * WIN, WIN), WIN)
        for pair in range(4):
            g = pair // 2
            qp = q_v[pl.ds(base, WIN), pair * WIN : (pair + 1) * WIN]
            acc = None
            peaks_now = []
            for side in range(2):
                s = scores(qp, kmask[g, side, keys_at, :]) + cut
                peak = jnp.maximum(
                    peaks[qt, pair, side], jnp.max(s, axis=1, keepdims=True)
                )
                expo = jnp.exp2((s - peak) * EXP_SCALE).astype(BF)
                o = jnp.dot(expo, vmask[g, side, keys_at, :], preferred_element_type=F32)
                acc = o if acc is None else acc + o
                peaks_now.append(peak)
            top = jnp.where(lane_low, peaks[qt, pair, 0], peaks[qt, pair, 1])
            peak = jnp.where(lane_low, peaks_now[0], peaks_now[1])
            logit = jnp.where(lane_low, sink[2 * pair], sink[2 * pair + 1]) * 8.0
            fade = jnp.exp2((top - peak) * EXP_SCALE)
            tail = jnp.exp2((logit - peak) * EXP_SCALE)
            div = near[qt, pair, :, WIN:] * fade + acc[:, WIN:] + tail
            att[pl.ds(base, WIN), pair * WIN : (pair + 1) * WIN] = (
                (near[qt, pair, :, 0:WIN] * fade + acc[:, 0:WIN]) / div
            ).astype(BF)

        @pl.when(step == 0)
        def _():
            send_att().start()

        return 0

    def send_att():
        return pltpu.make_async_remote_copy(
            att.at[pl.ds(pl.multiple_of(other * WIN, WIN), WIN)], attx, att_s, att_r,
            device_id=(me, other), device_id_type=MESH,
        )

    lax.fori_loop(0, 2, far_tile, 0)

    for i in (5, 6, 7):
        copies[i].wait()
    mine = pl.multiple_of(t * WIN, WIN)
    w_mine = pl.multiple_of(t * 512, 512)
    w_other = pl.multiple_of(other * 512, 512)
    for c in range(8):
        cols = slice(c * 256, (c + 1) * 256)
        midway[:, cols] = jnp.dot(
            att[pl.ds(mine, WIN), :], wout[pl.ds(w_mine, 512), cols], preferred_element_type=F32
        )
    send_att().wait()

    square = jnp.zeros((WIN, WIN), F32)
    for c in range(8):
        cols = slice(c * 256, (c + 1) * 256)
        proj = midway[:, cols] + jnp.dot(
            attx[...], wout[pl.ds(w_other, 512), cols], preferred_element_type=F32
        )
        mid = res[:, cols].astype(F32) + proj.astype(BF).astype(F32)
        midway[:, cols] = mid
        sq = mid * mid
        square = square + sq[:, 0:WIN] + sq[:, WIN:]
    inv = lax.rsqrt(jnp.sum(square, axis=1, keepdims=True) * (1.0 / DM) + EPSILON)
    for c in range(8):
        cols = slice(c * 256, (c + 1) * 256)
        normed[:, cols] = (midway[:, cols] * inv * gain[:, cols]).astype(BF)

    def tiles(count):
        return count * SLOT // TILE

    def dispatch(i):
        d = shifted(me, ORDER[i], 1)
        w = max(v for v in range(WAVES) if FIRST[v] <= i)
        shift = tiles(FIRST[w]) + t * tiles(SIZES[w])
        return [
            pltpu.make_async_remote_copy(
                xbuf3.at[tile, pl.ds(row, rows)], xin3.at[tile + shift, pl.ds(row, rows)],
                d_s, d_r.at[w], device_id=(d, t), device_id_type=MESH,
            )
            for tile, row, rows in pieces(i)
        ]

    def bulk(ref, count, send_sem, recv_sem):
        rows = ref.at[pl.ds(0, count), pl.ds(0, SLOT)]
        return pltpu.make_async_remote_copy(
            rows, rows, send_sem, recv_sem, device_id=(me, other), device_id_type=MESH
        )

    for w in range(WAVES):
        rows = slice(FIRST[w] * SLOT, (FIRST[w] + SIZES[w]) * SLOT)
        for c in range(8):
            cols = slice(c * 256, (c + 1) * 256)
            xbuf[rows, cols] = jnp.dot(
                disp[rows, :], normed[:, cols], preferred_element_type=F32
            ).astype(BF)
        for i in range(max(1, FIRST[w]), FIRST[w] + SIZES[w]):
            for copy in dispatch(i):
                copy.start()
    xin[pl.ds(pl.multiple_of(t * SIZES[0] * SLOT, TILE), SLOT), :] = xbuf[0:SLOT, :]
    weight = jnp.where(hits[0], rw[0:1, :], 0.0) + jnp.where(hits[1], rw[1:2, :], 0.0)
    for part_of in range(2):
        turned = weight[part_of * SLOTS // 2 : (part_of + 1) * SLOTS // 2].T
        high = turned.astype(BF)
        comb[part_of, 0] = high
        comb[part_of, 1] = (turned - high.astype(F32)).astype(BF)

    def wave_rows(w, side):
        return pl.multiple_of((2 * FIRST[w] + side * SIZES[w]) * SLOT, 8 * SLOT)

    def forward(w):
        rows = pl.ds(2 * tiles(FIRST[w]) + t * tiles(SIZES[w]), tiles(SIZES[w]))
        return pltpu.make_async_remote_copy(
            xin3.at[rows], xin3.at[rows], f_s.at[w], f_r.at[w],
            device_id=(me, other), device_id_type=MESH,
        )

    def halves(w):
        rows = pl.ds(wave_rows(w, other), SIZES[w] * SLOT)
        return pltpu.make_async_remote_copy(
            part.at[rows], recv.at[pl.ds(FIRST[w] * SLOT, SIZES[w] * SLOT)], p_s.at[w], p_r.at[w],
            device_id=(me, other), device_id_type=MESH,
        )

    def give_back(i):
        d = shifted(me, ORDER[i], -1)
        return [
            pltpu.make_async_remote_copy(
                back3.at[tile, pl.ds(row, rows)], ret3.at[tile, pl.ds(row, rows)],
                r_s, r_r.at[int(i >= NSP // 2)], device_id=(d, t), device_id_type=MESH,
            )
            for tile, row, rows in pieces(i)
        ]

    def arrive(w):
        bulk(xin3, SIZES[w] - (w == 0), d_s, d_r.at[w]).wait_recv()
        forward(w).start()

    def gate_up(w):
        forward(w).wait_recv()
        if w == 0:
            for i in (8, 9, 10):
                copies[i].wait()
        rows = slice(2 * FIRST[w] * SLOT, 2 * (FIRST[w] + SIZES[w]) * SLOT)
        for c in range(HID // 256):
            cols = slice(c * 256, (c + 1) * 256)
            gate = jnp.dot(xin[rows, :], wg[:, cols], preferred_element_type=F32)
            up = jnp.dot(xin[rows, :], wu[:, cols], preferred_element_type=F32)
            act = jnp.minimum(gate, CLAMP_LIMIT)
            lin = jnp.clip(up, -CLAMP_LIMIT, CLAMP_LIMIT) + 1.0
            hid[0 : 2 * SIZES[w] * SLOT, cols] = (lin * act * jax.nn.sigmoid(GATE_ALPHA * act)).astype(BF)

    def down(w):
        rows = slice(2 * FIRST[w] * SLOT, 2 * (FIRST[w] + SIZES[w]) * SLOT)
        for c in range(DM // 256):
            cols = slice(c * 256, (c + 1) * 256)
            part[rows, cols] = jnp.dot(
                hid[0 : 2 * SIZES[w] * SLOT, :], wd[:, cols], preferred_element_type=F32
            ).astype(BF)
        halves(w).start()

    def finish(w):
        halves(w).wait_recv()
        own = pl.ds(wave_rows(w, t), SIZES[w] * SLOT)
        rows = slice(FIRST[w] * SLOT, (FIRST[w] + SIZES[w]) * SLOT)
        for c in range(DM // 512):
            cols = slice(c * 512, (c + 1) * 512)
            back[rows, cols] = (
                part[own, cols].astype(F32) + recv[rows, cols].astype(F32)
            ).astype(BF)
        for i in range(max(1, FIRST[w]), FIRST[w] + SIZES[w]):
            for copy in give_back(i):
                copy.start()
        if w == 0:
            ret[0:SLOT, :] = back[0:SLOT, :]

    steps = {"a": arrive, "u": gate_up, "d": down, "f": finish}
    for step in PLAN:
        steps[step[0]](int(step[1:]))

    def combine(part_of):
        rows = slice(part_of * SLOTS // 2, (part_of + 1) * SLOTS // 2)
        for c in range(8):
            cols = slice(c * 256, (c + 1) * 256)
            total = midway[:, cols]
            for k in range(2):
                total = total + jnp.dot(
                    comb[part_of, k], ret[rows, cols], preferred_element_type=F32
                )
            if part_of == 1:
                out[:, cols] = total.astype(BF)
            else:
                midway[:, cols] = total

    bulk(xin3, NSP - 1, d_s, d_r.at[0]).wait_send()
    for w in range(WAVES):
        forward(w).wait_send()
        halves(w).wait_send()
    bulk(xin3, NSP // 2 - 1, r_s, r_r.at[0]).wait_recv()
    combine(0)
    bulk(xin3, NSP // 2, r_s, r_r.at[1]).wait_recv()
    combine(1)
    bulk(xin3, NSP - 1, r_s, r_r.at[0]).wait_send()


def per_device(
    queries, keys, values, sink_logit, w_out, residual, norm_gain, w_gate, w_up, w_down,
    expert_ids, route_weight,
):
    any_spec = pl.BlockSpec(memory_space=pltpu.HBM)
    specs = [any_spec] * 13
    code = [dz * 16 + dy * 4 + dx for dz, dy, dx in ORDER]
    rows = [c * 8 + j for c in code for j in range(SLOT)]
    table = np.array(rows, np.int32)[:, None].repeat(WIN, 1)
    dma = pltpu.SemaphoreType.DMA
    return pl.pallas_call(
        body,
        out_shape=pltpu.VMEM((WIN, DM), BF),
        in_specs=specs,
        out_specs=pl.BlockSpec(memory_space=pltpu.VMEM),
        scratch_shapes=[
            pltpu.VMEM((2 * WIN, 512), BF),
            pltpu.VMEM((2, 4 * WIN, WIN), BF),
            pltpu.VMEM((2, 2, 4 * WIN, WIN), BF),
            pltpu.VMEM((2, 2, 4 * WIN, 2 * WIN), BF),
            pltpu.VMEM((2, WIN, WIN), F32),
            pltpu.VMEM((2, 4, WIN, 2 * WIN), F32),
            pltpu.VMEM((2, 4, 2, WIN, WIN), F32),
            pltpu.VMEM((2 * WIN, 512), BF),
            pltpu.VMEM((WIN, 512), BF),
            pltpu.SMEM((8,), F32),
            pltpu.VMEM((1024, DM), BF),
            pltpu.VMEM((WIN, DM), BF),
            pltpu.VMEM((1, DM), F32),
            pltpu.VMEM((DM, HID), BF),
            pltpu.VMEM((DM, HID), BF),
            pltpu.VMEM((HID, DM), BF),
            pltpu.VMEM((2, WIN), jnp.int32),
            pltpu.VMEM((2, WIN), F32),
            pltpu.VMEM((SLOTS, WIN), jnp.int32),
            pltpu.VMEM((WIN, DM), F32),
            pltpu.VMEM((WIN, DM), BF),
            pltpu.VMEM((SLOTS, WIN), BF),
            pltpu.VMEM((2, 2, WIN, SLOTS // 2), BF),
            pltpu.VMEM((SLOTS // TILE, TILE, DM), BF),
            pltpu.VMEM((2 * SLOTS // TILE, TILE, DM), BF),
            pltpu.VMEM((2 * MOST * SLOT, HID), BF),
            pltpu.VMEM((2 * SLOTS, DM), BF),
            pltpu.VMEM((SLOTS, DM), BF),
            pltpu.VMEM((SLOTS // TILE, TILE, DM), BF),
            pltpu.VMEM((SLOTS // TILE, TILE, DM), BF),
            dma((13,)),
            dma((2,)),
            dma((2,)),
            dma,
            dma,
            dma,
            dma((WAVES,)),
            dma((WAVES,)),
            dma((WAVES,)),
            dma((WAVES,)),
            dma((WAVES,)),
            dma,
            dma((2,)),
        ],
        compiler_params=pltpu.CompilerParams(
            collective_id=0, has_side_effects=True, vmem_limit_bytes=58 * 2**20
        ),
    )(
        queries, keys, values, sink_logit, w_out, residual, norm_gain.reshape(1, DM),
        w_gate[0], w_up[0], w_down[0], expert_ids.T, route_weight.T, jnp.asarray(table),
    )


def solution(mesh):
    in_specs = (
        P("sp", "tp"),
        P("sp", "tp"),
        P("sp", "tp"),
        P("tp"),
        P(),
        P(("sp", "tp"), None),
        P(),
        P("sp", None, "tp"),
        P("sp", None, "tp"),
        P("sp", "tp", None),
        P(("sp", "tp"), None),
        P(("sp", "tp"), None),
    )
    return jax.shard_map(
        per_device,
        mesh=mesh,
        in_specs=in_specs,
        out_specs=P(("sp", "tp"), None),
        check_vma=False,
    )
```

time: 67.9 us -> 58.9 us (0.87); the launches traced: 66.8 us -> 58.8 us
  Pallas kernels: 64.9 us -> 58 us
  local copies, waits for them, and re-layouts: 1.88 us -> 0.8 us
    pallas_call x1, Pallas kernels: 64.9 us -> 58 us  [per_device(): pl.pallas_call(body, out_shape=pltpu.VMEM((WIN, DM), BF), in_specs=specs,...]
    unnamed x1, local copies, waits for them, and re-layouts: 1.88 us -> 0.8 us
where the time goes in v2:
time: 58.9 us; the launch traced here: 58.8 us
  Pallas kernels  58 us (98%)
  local copies, waits for them, and re-layouts  0.8 us (1%)
    pallas_call x1, Pallas kernels, per_device(): pl.pallas_call(body, out_shape=pltpu.VMEM((WIN, DM), BF), in_specs=specs,...  58 us

profile of v2, /device:TPU:1, one launch (start us, length us, event | category | flops | bytes accessed | tf_op | source)
XLA Modules:
  0.0 58.8 jit_solution(7274356445210953135)
XLA Ops:
  0.0 58.0 %shard_map.127 = bf16[128,2048]{1,0:T(8,128)(2,1)S(1)} custom-call(bf16[256,512]{1,0:T(8,128)(2,1)} %q_hbm.1, bf16[256,128]{1,0:T(8,128)(2,1)} %k_hbm.1, bf16[256,128]{1,0:T(8,128)(2,1)} %v_hbm.1, f32[8]{0:T(128)} %sink_hbm.1, bf16[1024,2048]{1,0:T(8,128)(2,1)} %wout_hbm.1, bf16[128,2048]{1,0:T(8,128)(2,1)} %res_hbm.1, f32[1,2048]{1,0:T(1,128)} %bitcast.9, ...), custom_call_target="tpu_custom_call" | custom-call | tf_op jit(solution)/shard_map/pallas_call | solution.py:442
  58.0 0.8 %copy.15 = bf16[128,2048]{1,0:T(8,128)(2,1)} copy(bf16[128,2048]{1,0:T(8,128)(2,1)S(1)} %shard_map.127) | data formatting | bytes 1048576

commit v3 on v2

--- a/solution.py
+++ b/solution.py
@@ -23,7 +23,7 @@
 WAVES = len(SIZES)
 PLAN = (
     "a0", "u0", "a1", "d0", "u1", "f0", "a2", "d1", "a3", "u2",
-    "f1", "a4", "d2", "u3", "f2", "d3", "u4", "f3", "d4", "f4",
+    "f1", "d2", "a4", "u3", "f2", "d3", "u4", "f3", "d4", "f4",
 )
 FIRST = [sum(SIZES[:w]) for w in range(WAVES)]
 MOST = max(SIZES)

time: 58.9 us -> 59 us (level)
  no operation moved by 1% of the time
where the time goes in v3:
time: 59 us; the launch traced here: 58.9 us
  Pallas kernels  58.1 us (98%)
  local copies, waits for them, and re-layouts  0.8 us (1%)
    pallas_call x1, Pallas kernels, per_device(): pl.pallas_call(body, out_shape=pltpu.VMEM((WIN, DM), BF), in_specs=specs,...  58.1 us

profile of v3, /device:TPU:1, one launch (start us, length us, event | category | flops | bytes accessed | tf_op | source)
XLA Modules:
  0.0 58.9 jit_solution(6075996499150614202)
XLA Ops:
  0.0 58.1 %shard_map.127 = bf16[128,2048]{1,0:T(8,128)(2,1)S(1)} custom-call(bf16[256,512]{1,0:T(8,128)(2,1)} %q_hbm.1, bf16[256,128]{1,0:T(8,128)(2,1)} %k_hbm.1, bf16[256,128]{1,0:T(8,128)(2,1)} %v_hbm.1, f32[8]{0:T(128)} %sink_hbm.1, bf16[1024,2048]{1,0:T(8,128)(2,1)} %wout_hbm.1, bf16[128,2048]{1,0:T(8,128)(2,1)} %res_hbm.1, f32[1,2048]{1,0:T(1,128)} %bitcast.9, ...), custom_call_target="tpu_custom_call" | custom-call | tf_op jit(solution)/shard_map/pallas_call | solution.py:442
  58.1 0.8 %copy.15 = bf16[128,2048]{1,0:T(8,128)(2,1)} copy(bf16[128,2048]{1,0:T(8,128)(2,1)S(1)} %shard_map.127) | data formatting | bytes 1048576

commit v4 on v3

--- a/solution.py
+++ b/solution.py
@@ -28,6 +28,7 @@
 FIRST = [sum(SIZES[:w]) for w in range(WAVES)]
 MOST = max(SIZES)
 SLOTS = NSP * SLOT
+STAGES = (0, 32, 48, 64)
 
 
 def pieces(i):
@@ -325,11 +326,13 @@
                 copy.start()
     xin[pl.ds(pl.multiple_of(t * SIZES[0] * SLOT, TILE), SLOT), :] = xbuf[0:SLOT, :]
     weight = jnp.where(hits[0], rw[0:1, :], 0.0) + jnp.where(hits[1], rw[1:2, :], 0.0)
-    for part_of in range(2):
-        turned = weight[part_of * SLOTS // 2 : (part_of + 1) * SLOTS // 2].T
+    for stage in range(3):
+        rows = slice(STAGES[stage] * SLOT, STAGES[stage + 1] * SLOT)
+        size = rows.stop - rows.start
+        turned = weight[rows].T
         high = turned.astype(BF)
-        comb[part_of, 0] = high
-        comb[part_of, 1] = (turned - high.astype(F32)).astype(BF)
+        comb[stage, 0, :, 0:size] = high
+        comb[stage, 1, :, 0:size] = (turned - high.astype(F32)).astype(BF)
 
     def wave_rows(w, side):
         return pl.multiple_of((2 * FIRST[w] + side * SIZES[w]) * SLOT, 8 * SLOT)
@@ -353,7 +356,7 @@
         return [
             pltpu.make_async_remote_copy(
                 back3.at[tile, pl.ds(row, rows)], ret3.at[tile, pl.ds(row, rows)],
-                r_s, r_r.at[int(i >= NSP // 2)], device_id=(d, t), device_id_type=MESH,
+                r_s, r_r.at[int(i >= STAGES[1]) + int(i >= STAGES[2])], device_id=(d, t), device_id_type=MESH,
             )
             for tile, row, rows in pieces(i)
         ]
@@ -405,15 +408,16 @@
         steps[step[0]](int(step[1:]))
 
     def combine(part_of):
-        rows = slice(part_of * SLOTS // 2, (part_of + 1) * SLOTS // 2)
+        rows = slice(STAGES[part_of] * SLOT, STAGES[part_of + 1] * SLOT)
+        size = rows.stop - rows.start
         for c in range(8):
             cols = slice(c * 256, (c + 1) * 256)
             total = midway[:, cols]
             for k in range(2):
                 total = total + jnp.dot(
-                    comb[part_of, k], ret[rows, cols], preferred_element_type=F32
+                    comb[part_of, k, :, 0:size], ret[rows, cols], preferred_element_type=F32
                 )
-            if part_of == 1:
+            if part_of == 2:
                 out[:, cols] = total.astype(BF)
             else:
                 midway[:, cols] = total
@@ -422,10 +426,10 @@
     for w in range(WAVES):
         forward(w).wait_send()
         halves(w).wait_send()
-    bulk(xin3, NSP // 2 - 1, r_s, r_r.at[0]).wait_recv()
-    combine(0)
-    bulk(xin3, NSP // 2, r_s, r_r.at[1]).wait_recv()
-    combine(1)
+    for stage in range(3):
+        count = STAGES[stage + 1] - STAGES[stage] - (stage == 0)
+        bulk(xin3, count, r_s, r_r.at[stage]).wait_recv()
+        combine(stage)
     bulk(xin3, NSP - 1, r_s, r_r.at[0]).wait_send()
 
 
@@ -467,7 +471,7 @@
             pltpu.VMEM((WIN, DM), F32),
             pltpu.VMEM((WIN, DM), BF),
             pltpu.VMEM((SLOTS, WIN), BF),
-            pltpu.VMEM((2, 2, WIN, SLOTS // 2), BF),
+            pltpu.VMEM((3, 2, WIN, SLOTS // 2), BF),
             pltpu.VMEM((SLOTS // TILE, TILE, DM), BF),
             pltpu.VMEM((2 * SLOTS // TILE, TILE, DM), BF),
             pltpu.VMEM((2 * MOST * SLOT, HID), BF),
@@ -487,7 +491,7 @@
             dma((WAVES,)),
             dma((WAVES,)),
             dma,
-            dma((2,)),
+            dma((3,)),
         ],
         compiler_params=pltpu.CompilerParams(
             collective_id=0, has_side_effects=True, vmem_limit_bytes=58 * 2**20

time: 59 us -> 59 us (level)
  no operation moved by 1% of the time
where the time goes in v4:
time: 59 us; the launch traced here: 58.9 us
  Pallas kernels  58.1 us (98%)
  local copies, waits for them, and re-layouts  0.8 us (1%)
    pallas_call x1, Pallas kernels, per_device(): pl.pallas_call(body, out_shape=pltpu.VMEM((WIN, DM), BF), in_specs=specs,...  58.1 us

profile of v4, /device:TPU:1, one launch (start us, length us, event | category | flops | bytes accessed | tf_op | source)
XLA Modules:
  0.0 58.9 jit_solution(15122262327394736610)
XLA Ops:
  0.0 58.1 %shard_map.127 = bf16[128,2048]{1,0:T(8,128)(2,1)S(1)} custom-call(bf16[256,512]{1,0:T(8,128)(2,1)} %q_hbm.1, bf16[256,128]{1,0:T(8,128)(2,1)} %k_hbm.1, bf16[256,128]{1,0:T(8,128)(2,1)} %v_hbm.1, f32[8]{0:T(128)} %sink_hbm.1, bf16[1024,2048]{1,0:T(8,128)(2,1)} %wout_hbm.1, bf16[128,2048]{1,0:T(8,128)(2,1)} %res_hbm.1, f32[1,2048]{1,0:T(1,128)} %bitcast.9, ...), custom_call_target="tpu_custom_call" | custom-call | tf_op jit(solution)/shard_map/pallas_call | solution.py:446
  58.1 0.8 %copy.15 = bf16[128,2048]{1,0:T(8,128)(2,1)} copy(bf16[128,2048]{1,0:T(8,128)(2,1)S(1)} %shard_map.127) | data formatting | bytes 1048576
